TPU v7x, 32 devices: a whole 2x2x4 slice. The times are simulated.
32 devices in a mesh: sp: 16 (over z, y, x), tp: 2 (over core).
Axes of the slice: x: 2, y: 2, z: 4, core: 2. Of those that a mesh axis runs over, the one named last changes fastest.
Arguments:
- tokens: bfloat16 [4096, 2048], P('sp', 'tp'), may hold values from -12 to 12
- norm_gain: float32 [2048], replicated, may hold values from 0.1 to 1.9
- window_query: bfloat16 [2048, 1024], P(None, 'tp'), may hold values from -2 to 2
- window_key: bfloat16 [2048, 512], P(None, 'tp'), may hold values from -2 to 2
- window_value: bfloat16 [2048, 512], P(None, 'tp'), may hold values from -0.125 to 0.125
- window_gate: bfloat16 [2048, 1024], P(None, 'tp'), may hold values from -0.125 to 0.125
- window_sink: float32 [16], P('tp'), may hold values from 2 to 6
- pair_query: bfloat16 [2048, 1024], P(None, 'tp'), may hold values from -2 to 2
- pair_key: bfloat16 [2048, 1024], P(None, 'tp'), may hold values from -2 to 2
- pair_value: bfloat16 [2048, 1024], P(None, 'tp'), may hold values from -0.125 to 0.125
- pair_gate: bfloat16 [2048, 1024], P(None, 'tp'), may hold values from -0.125 to 0.125
- map_lambda: float32 [8], P('tp'), may hold values from 0.3 to 0.8
- head_gain: float32 [128], replicated, may hold values from 0.1 to 1.9
- window_out: bfloat16 [1024, 2048], P('tp'), may hold values from -0.125 to 0.125
- pair_out: bfloat16 [1024, 2048], P('tp'), may hold values from -0.125 to 0.125
Outputs:
- mixed: bfloat16 [4096, 2048], P(('sp', 'tp'))
All inputs are finite; a program needn't handle non-finite values.
Results may differ from a plain program's by a relative error of at most 0.018.
Values may be sent and summed in bfloat16 or wider, within the bound.
A program may use at most 128 MiB of HBM per device.

v0:
```python
import functools
import math

import jax
import jax.numpy as jnp
from jax import lax
from jax.experimental import pallas as pl
from jax.experimental.pallas import tpu as pltpu
from jax.sharding import PartitionSpec as P

HD = 64
WINDOW = 128

norm_eps = 1e-06
head_scale = 0.8

MESH = pl.DeviceIdType.MESH
F32 = jnp.float32
BF16 = jnp.bfloat16


def dot_nt(a, b):
    return lax.dot_general(a, b, (((1,), (1,)), ((), ())), preferred_element_type=F32)


def dot_tn(a, b):
    return lax.dot_general(a, b, (((0,), (0,)), ((), ())), preferred_element_type=F32)


def silu(v):
    return v / (1.0 + jnp.exp(-v))


def kernel(
    S,
    T,
    tokens,
    norm_gain,
    wq_h,
    wk_h,
    wv_h,
    wg_h,
    sink,
    pq_h,
    pk_h,
    pv_h,
    pg_h,
    lam,
    head_gain,
    wo_h,
    po_h,
    out,
    wq,
    wk,
    wv,
    wg,
    pq,
    pk,
    pv,
    pg,
    wo,
    po,
    tok_buf,
    normed,
    band_k,
    band_v,
    sq_buf,
    sg_buf,
    pg_buf,
    slide_mix,
    paired_mix,
    kv_send,
    q_send,
    kv_all,
    q_all,
    q2_buf,
    m_buf,
    l_buf,
    acc_buf,
    ret_send,
    ret_all,
    part,
    part_bf,
    rs_buf,
    w_sem,
    tok_s,
    tok_r,
    kv1_s,
    kv2_s,
    kv_r,
    q_s,
    q_r,
    tail_s,
    tail_r,
    ret_s,
    ret_r,
    rs_s,
    rs_r,
):
    R = tokens.shape[0]
    Dl = tokens.shape[1]
    D = Dl * T
    G = kv_send.shape[0]
    M = S // G
    C = kv_send.shape[3]
    Hg = C // (2 * HD)
    s = lax.axis_index("sp")
    t = lax.axis_index("tp")
    g = s // M
    m = lax.rem(s, M)

    pairs = [(pk_h, pk), (pv_h, pv), (pq_h, pq), (wk_h, wk), (wv_h, wv), (wq_h, wq), (wg_h, wg), (pg_h, pg), (wo_h, wo), (po_h, po)]
    loads = [pltpu.make_async_copy(a, b, w_sem.at[i]) for i, (a, b) in enumerate(pairs)]
    for cp in loads:
        cp.start()

    barrier = pltpu.get_barrier_semaphore()
    for dt in range(1, T):
        pl.semaphore_signal(barrier, inc=1, device_id={"tp": lax.rem(t + dt, T)}, device_id_type=MESH)

    def greet(d, _):
        pl.semaphore_signal(barrier, inc=1, device_id={"sp": lax.rem(s + d, S)}, device_id_type=MESH)
        return 0

    lax.fori_loop(1, S, greet, 0)
    tok_buf[t] = tokens[...]
    pl.semaphore_wait(barrier, S + T - 2)

    def tok_copy(dt):
        return pltpu.make_async_remote_copy(
            tokens,
            tok_buf.at[t],
            tok_s.at[dt],
            tok_r.at[dt],
            device_id={"tp": lax.rem(t + dt, T)},
            device_id_type=MESH,
        )

    def tok_in(dt):
        return pltpu.make_async_remote_copy(
            tokens,
            tok_buf.at[lax.rem(t + T - dt, T)],
            tok_s.at[dt],
            tok_r.at[dt],
            device_id={"tp": lax.rem(t + dt, T)},
            device_id_type=MESH,
        )

    for dt in range(1, T):
        tok_copy(dt).start()
    for dt in range(1, T):
        tok_in(dt).wait_recv()

    NB = 32

    def norm_rows(i, _):
        rows = pl.ds(pl.multiple_of(i * NB, NB), NB)
        xs = [tok_buf[k, rows, :].astype(F32) for k in range(T)]
        total = sum(jnp.sum(x * x, axis=-1, keepdims=True) for x in xs)
        r = lax.rsqrt(total * (1.0 / D) + norm_eps)
        for k in range(T):
            cols = slice(k * Dl, (k + 1) * Dl)
            normed[rows, cols] = (xs[k] * r * norm_gain[:, cols]).astype(BF16)
        return 0

    lax.fori_loop(0, R // NB, norm_rows, 0)

    def project(i, store):
        loads[i].wait()
        w = pairs[i][1]
        cols = w.shape[1]
        tile = min(256, cols)
        for c in range(0, cols, tile):
            r = jnp.dot(normed[...], w[:, c : c + tile], preferred_element_type=F32).astype(BF16)
            store(c, tile, r)

    def grouped(write):
        def store(c, tile, r):
            for o in range(0, tile, 2 * HD):
                at = c + o
                write(at // C, at % C, r[:, o : o + 2 * HD])

        return store

    def put_k(gi, col, r):
        kv_send[gi, 0, :, col : col + 2 * HD] = r

    def put_v(gi, col, r):
        kv_send[gi, 1, :, col : col + 2 * HD] = r

    def put_q(gi, col, r):
        q_send[gi, :, col : col + 2 * HD] = r

    def plane(gi, mi):
        return {"sp": gi * M + mi}

    def kv1(dg):
        return pltpu.make_async_remote_copy(
            kv_send.at[lax.rem(g + dg, G)],
            kv_all.at[s],
            kv1_s.at[dg],
            kv_r.at[dg * M],
            device_id=plane(lax.rem(g + dg, G), m),
            device_id_type=MESH,
        )

    def source(dg, dm):
        return lax.rem(g + G - dg, G) * M + lax.rem(m + M - dm, M)

    def kv_in(dg, dm):
        at = kv_all.at[source(dg, dm)]
        return pltpu.make_async_remote_copy(
            at,
            at,
            kv2_s.at[dg * M + dm],
            kv_r.at[dg * M + dm],
            device_id=plane(g, lax.rem(m + 1, M)),
            device_id_type=MESH,
        )

    def kv2(dg, dm):
        at = kv_all.at[source(dg, 0)]
        return pltpu.make_async_remote_copy(
            at,
            at,
            kv2_s.at[dg * M + dm],
            kv_r.at[dg * M + dm],
            device_id=plane(g, lax.rem(m + dm, M)),
            device_id_type=MESH,
        )

    def forward(dg):
        def one(dm, _):
            kv2(dg, dm).start()
            return 0

        lax.fori_loop(1, M, one, 0)

    def q_copy(dg):
        return pltpu.make_async_remote_copy(
            q_send.at[lax.rem(g + dg, G)],
            q_all.at[g],
            q_s.at[dg],
            q_r.at[dg],
            device_id=plane(lax.rem(g + dg, G), m),
            device_id_type=MESH,
        )

    def q_in(dg):
        return pltpu.make_async_remote_copy(
            q_send.at[0],
            q_all.at[lax.rem(g + G - dg, G)],
            q_s.at[dg],
            q_r.at[dg],
            device_id=plane(lax.rem(g + dg, G), m),
            device_id_type=MESH,
        )

    project(0, grouped(put_k))
    project(1, grouped(put_v))
    for dg in range(1, G):
        kv1(dg).start()
    kv_all[s] = kv_send[g]
    forward(0)
    project(2, grouped(put_q))
    for dg in range(1, G):
        q_copy(dg).start()
    q_all[g] = q_send[g]

    def into(ref, first=0):
        def store(c, tile, r):
            ref[first:, c : c + tile] = r

        return store

    project(3, into(band_k, WINDOW))
    project(4, into(band_v, WINDOW))

    def tails():
        nxt = {"sp": lax.rem(s + 1, S)}
        return [
            pltpu.make_async_remote_copy(
                b.at[pl.ds(R, WINDOW)],
                b.at[pl.ds(0, WINDOW)],
                tail_s.at[i],
                tail_r.at[i],
                device_id=nxt,
                device_id_type=MESH,
            )
            for i, b in enumerate((band_k, band_v))
        ]

    @pl.when(s < S - 1)
    def _():
        for cp in tails():
            cp.start()

    @pl.when(s == 0)
    def _():
        band_k[0:WINDOW] = jnp.zeros((WINDOW, band_k.shape[1]), BF16)
        band_v[0:WINDOW] = jnp.zeros((WINDOW, band_v.shape[1]), BF16)

    def relay(dg):
        if dg < G:
            kv_in(dg, 0).wait_recv()
            forward(dg)

    project(5, into(sq_buf))
    project(6, into(sg_buf))
    relay(1)
    project(7, into(pg_buf))
    relay(2)

    @pl.when(s > 0)
    def _():
        for cp in tails():
            cp.wait_recv()

    scale = HD**-0.5
    kv_heads = band_k.shape[1] // HD
    group = sq_buf.shape[1] // band_k.shape[1]
    W = WINDOW
    blocks = R // W
    key_i = lax.broadcasted_iota(jnp.int32, (2 * W, group * W), 0)
    qry_i = lax.rem(lax.broadcasted_iota(jnp.int32, (2 * W, group * W), 1), W)
    lane_head = lax.broadcasted_iota(jnp.int32, (1, group * W), 1) // W
    dist = qry_i - key_i + W
    in_band = (dist >= 0) & (dist < W)

    def window_block(b):
        r0 = b * W
        ok = in_band & (s * R + r0 - W + key_i >= 0)
        for h in range(kv_heads):
            k = band_k[r0 : r0 + 2 * W, h * HD : (h + 1) * HD]
            v = band_v[r0 : r0 + 2 * W, h * HD : (h + 1) * HD]
            q = jnp.concatenate(
                [sq_buf[r0 : r0 + W, (h * group + e) * HD : (h * group + e + 1) * HD] for e in range(group)], axis=0
            )
            sc = jnp.where(ok, dot_nt(k, q) * scale, -jnp.inf)
            sk = jnp.full((1, group * W), sink[0, h * group], F32)
            for e in range(1, group):
                sk = jnp.where(lane_head == e, sink[0, h * group + e], sk)
            top = jnp.maximum(jnp.max(sc, axis=0, keepdims=True), sk)
            w = jnp.exp(sc - top)
            den = jnp.sum(w, axis=0, keepdims=True) + jnp.exp(sk - top)
            probs = (w * (1.0 / den)).astype(BF16)
            o = dot_tn(v, probs)
            o = jnp.concatenate([o[:, e * W : (e + 1) * W] for e in range(group)], axis=0).T
            cols = slice(h * group * HD, (h + 1) * group * HD)
            gate = sg_buf[r0 : r0 + W, cols].astype(F32)
            slide_mix[r0 : r0 + W, cols] = (o * silu(gate)).astype(BF16)

    for b in range(blocks):
        window_block(b)
        if b == 0:
            relay(3)
    for dg in range(4, G):
        relay(dg)

    for dg in range(1, G):
        q_in(dg).wait_recv()
    lane = lax.broadcasted_iota(jnp.int32, (R, 2 * HD), 1)
    for gi in range(G):
        for j in range(Hg):
            q = q_all[gi, :, j * 2 * HD : (j + 1) * 2 * HD].astype(F32) * scale
            q2_buf[gi, j, 0:R, :] = jnp.where(lane < HD, q, 0.0).astype(BF16)
            q2_buf[gi, j, R:, :] = jnp.where(lane < HD, 0.0, q).astype(BF16)
    m_buf[...] = jnp.full(m_buf.shape, -1e30, F32)
    l_buf[...] = jnp.zeros(l_buf.shape, F32)
    acc_buf[...] = jnp.zeros(acc_buf.shape, F32)

    def update(at, gi, masked):
        for j in range(Hg):
            cols = slice(j * 2 * HD, (j + 1) * 2 * HD)
            st = dot_nt(kv_all[at, 0, :, cols], q2_buf[gi, j])
            if masked:
                ki = lax.broadcasted_iota(jnp.int32, (R, 2 * R), 0)
                qi = lax.rem(lax.broadcasted_iota(jnp.int32, (R, 2 * R), 1), R)
                st = jnp.where(qi >= ki, st, -jnp.inf)
            old = m_buf[gi, j]
            new = jnp.maximum(old, jnp.max(st, axis=0, keepdims=True))
            f = jnp.exp(old - new)
            p = jnp.exp(st - new)
            m_buf[gi, j] = new
            l_buf[gi, j] = l_buf[gi, j] * f + jnp.sum(p, axis=0, keepdims=True)
            acc_buf[gi, j] = acc_buf[gi, j] * f + dot_tn(kv_all[at, 1, :, cols], p.astype(BF16))

    def process(at):
        def one(gi, _):
            mine = gi * M + m

            @pl.when(at < mine)
            def _():
                update(at, gi, False)

            @pl.when(at == mine)
            def _():
                update(at, gi, True)

            return 0

        lax.fori_loop(0, G, one, 0)

    def near(dg, _):
        process(source(dg, 0))
        return 0

    lax.fori_loop(0, G, near, 0)

    def far(i, _):
        dg = i // (M - 1)
        dm = 1 + lax.rem(i, M - 1)
        kv_in(dg, dm).wait_recv()
        process(source(dg, dm))
        return 0

    if M > 1:
        lax.fori_loop(0, G * (M - 1), far, 0)

    def ret_copy(dg):
        return pltpu.make_async_remote_copy(
            ret_send.at[lax.rem(g + dg, G)],
            ret_all.at[g],
            ret_s.at[dg],
            ret_r.at[dg],
            device_id=plane(lax.rem(g + dg, G), m),
            device_id_type=MESH,
        )

    def ret_in(dg):
        return pltpu.make_async_remote_copy(
            ret_send.at[0],
            ret_all.at[lax.rem(g + G - dg, G)],
            ret_s.at[dg],
            ret_r.at[dg],
            device_id=plane(lax.rem(g + dg, G), m),
            device_id_type=MESH,
        )

    def finish(gi):
        for j in range(Hg):
            a = acc_buf[gi, j] * (1.0 / l_buf[gi, j])
            d = a[:, 0:R] - lam[0, g * Hg + j] * a[:, R:]
            sq = jnp.mean(d * d, axis=0, keepdims=True)
            y = (d * (lax.rsqrt(sq + norm_eps) * head_scale)).T * head_gain[...]
            ret_send[gi, :, j * 2 * HD : (j + 1) * 2 * HD] = y.astype(BF16)

    for dg in range(1, G):
        finish(lax.rem(g + dg, G))
        ret_copy(dg).start()
    finish(g)
    ret_all[g] = ret_send[g]

    loads[8].wait()
    NT = min(512, D)
    for c in range(0, D, NT):
        part[:, c : c + NT] = jnp.dot(slide_mix[...], wo[:, c : c + NT], preferred_element_type=F32)
    for dg in range(1, G):
        ret_in(dg).wait_recv()
    for gi in range(G):
        gate = pg_buf[:, gi * C : (gi + 1) * C].astype(F32)
        paired_mix[:, gi * C : (gi + 1) * C] = (ret_all[gi].astype(F32) * silu(gate)).astype(BF16)
    loads[9].wait()
    Rt = R // T
    for c in range(0, D, NT):
        r = part[:, c : c + NT] + jnp.dot(paired_mix[...], po[:, c : c + NT], preferred_element_type=F32)
        r = r.astype(BF16)
        for k in range(T):
            part_bf[k, :, c : c + NT] = r[k * Rt : (k + 1) * Rt]

    def rs_copy(dt):
        return pltpu.make_async_remote_copy(
            part_bf.at[lax.rem(t + dt, T)],
            rs_buf.at[dt],
            rs_s.at[dt],
            rs_r.at[dt],
            device_id={"tp": lax.rem(t + dt, T)},
            device_id_type=MESH,
        )

    for dt in range(1, T):
        rs_copy(dt).start()
    for dt in range(1, T):
        rs_copy(dt).wait_recv()
    for c in range(0, D, NT):
        total = part_bf[t, :, c : c + NT].astype(F32)
        for dt in range(1, T):
            total = total + rs_buf[dt, :, c : c + NT].astype(F32)
        out[:, c : c + NT] = total.astype(BF16)

    for dt in range(1, T):
        tok_copy(dt).wait_send()
        rs_copy(dt).wait_send()
    for dg in range(1, G):
        kv1(dg).wait_send()
        q_copy(dg).wait_send()
        ret_copy(dg).wait_send()

    def drain(i, _):
        kv2(i // (M - 1), 1 + lax.rem(i, M - 1)).wait_send()
        return 0

    if M > 1:
        lax.fori_loop(0, G * (M - 1), drain, 0)

    @pl.when(s < S - 1)
    def _():
        for cp in tails():
            cp.wait_send()


def per_device(S, T, tokens, norm_gain, wq, wk, wv, wg, sink, pq, pk, pv, pg, lam, head_gain, wo, po):
    R, Dl = tokens.shape
    D = Dl * T
    A = wq.shape[1]
    KC = wk.shape[1]
    B = pq.shape[1]
    H = B // (2 * HD)
    G = math.gcd(H, S)
    Hg = H // G
    C = Hg * 2 * HD
    vmem = pl.BlockSpec(memory_space=pltpu.VMEM)
    smem = pl.BlockSpec(memory_space=pltpu.SMEM)
    hbm = pl.BlockSpec(memory_space=pl.ANY)
    dma = pltpu.SemaphoreType.DMA
    V = pltpu.VMEM
    scratch = [V(w.shape, BF16) for w in (wq, wk, wv, wg, pq, pk, pv, pg, wo, po)]
    scratch += [
        V((T, R, Dl), BF16),
        V((R, D), BF16),
        V((WINDOW + R, KC), BF16),
        V((WINDOW + R, KC), BF16),
        V((R, A), BF16),
        V((R, A), BF16),
        V((R, B), BF16),
        V((R, A), BF16),
        V((R, B), BF16),
        V((G, 2, R, C), BF16),
        V((G, R, C), BF16),
        V((S, 2, R, C), BF16),
        V((G, R, C), BF16),
        V((G, Hg, 2 * R, 2 * HD), BF16),
        V((G, Hg, 1, 2 * R), F32),
        V((G, Hg, 1, 2 * R), F32),
        V((G, Hg, 2 * HD, 2 * R), F32),
        V((G, R, C), BF16),
        V((G, R, C), BF16),
        V((R, D), F32),
        V((T, R // T, D), BF16),
        V((T, R // T, D), BF16),
        dma((10,)),
        dma((T,)),
        dma((T,)),
        dma((G,)),
        dma((S,)),
        dma((S,)),
        dma((G,)),
        dma((G,)),
        dma((2,)),
        dma((2,)),
        dma((G,)),
        dma((G,)),
        dma((T,)),
        dma((T,)),
    ]
    return pl.pallas_call(
        functools.partial(kernel, S, T),
        out_shape=jax.ShapeDtypeStruct((R // T, D), BF16),
        in_specs=[vmem, vmem, hbm, hbm, hbm, hbm, smem, hbm, hbm, hbm, hbm, smem, vmem, hbm, hbm],
        out_specs=vmem,
        scratch_shapes=scratch,
        compiler_params=pltpu.CompilerParams(
            collective_id=0, has_side_effects=True, vmem_limit_bytes=60 * 1024 * 1024
        ),
        name="layer",
    )(
        tokens,
        norm_gain.reshape(1, D),
        wq,
        wk,
        wv,
        wg,
        sink.reshape(1, -1),
        pq,
        pk,
        pv,
        pg,
        lam.reshape(1, -1),
        head_gain.reshape(1, -1),
        wo,
        po,
    )


def solution(mesh):
    S, T = mesh.shape["sp"], mesh.shape["tp"]
    in_specs = (
        P("sp", "tp"),
        P(),
        P(None, "tp"),
        P(None, "tp"),
        P(None, "tp"),
        P(None, "tp"),
        P("tp"),
        P(None, "tp"),
        P(None, "tp"),
        P(None, "tp"),
        P(None, "tp"),
        P("tp"),
        P(),
        P("tp", None),
        P("tp", None),
    )
    return jax.shard_map(
        functools.partial(per_device, S, T),
        mesh=mesh,
        in_specs=in_specs,
        out_specs=P(("sp", "tp"), None),
        check_vma=False,
    )
```

profile of v0, /device:TPU:1, one launch (start us, length us, event | category | flops | bytes accessed | tf_op | source)
XLA Modules:
  0.0 62.6 jit_solution(3357907254646732609)
XLA Ops:
  0.0 60.7 %layer.1 = bf16[128,2048]{1,0:T(8,128)(2,1)} custom-call(bf16[256,1024]{1,0:T(8,128)(2,1)} %tokens.1, f32[1,2048]{1,0:T(1,128)} %bitcast.4, bf16[2048,512]{1,0:T(8,128)(2,1)} %wq_h.1, bf16[2048,256]{1,0:T(8,128)(2,1)} %wk_h.1, bf16[2048,256]{1,0:T(8,128)(2,1)} %wv_h.1, bf16[2048,512]{1,0:T(8,128)(2,1)} %wg_h.1, f32[1,8]{1,0:T(1,128)} %bitcast.5, ...), custom_call_target="tpu_custom_call" | custom-call | tf_op jit(solution)/shard_map/layer/pallas_call | solution.py:566
  60.7 1.9 %copy.17 = bf16[128,2048]{1,0:T(8,128)(2,1)} copy(bf16[128,2048]{1,0:T(8,128)(2,1)} %layer.1) | data formatting | bytes 1048576
where the time goes:
time: 62.8 us; the launch traced here: 62.6 us
  Pallas kernels  60.7 us (97%)
  local copies, waits for them, and re-layouts  1.88 us (3%)
    pallas_call x1, Pallas kernels, per_device(): pl.pallas_call(functools.partial(kernel, S, T), out_shape=jax.ShapeDtypeS...  60.7 us
    unnamed x1, local copies, waits for them, and re-layouts  1.88 us

commit v1 on v0

v1 whole, which is shorter than its diff:
```python
import functools

import jax
import jax.numpy as jnp
from jax import lax
from jax.experimental import pallas as pl
from jax.experimental.pallas import tpu as pltpu
from jax.sharding import PartitionSpec as P

HD = 64
WINDOW = 128

norm_eps = 1e-06
head_scale = 0.8
CHUNK = 8
ONES = 16

MESH = pl.DeviceIdType.MESH
F32 = jnp.float32
BF16 = jnp.bfloat16


def dot_nt(a, b):
    return lax.dot_general(a, b, (((1,), (1,)), ((), ())), preferred_element_type=F32)


def dot_tn(a, b):
    return lax.dot_general(a, b, (((0,), (0,)), ((), ())), preferred_element_type=F32)


def silu(v):
    return v / (1.0 + jnp.exp(-v))


def kernel(
    S,
    T,
    tokens,
    gain_h,
    wq_h,
    wk_h,
    wv_h,
    wg_h,
    sink,
    pq_h,
    pk_h,
    pv_h,
    pg_h,
    lam_h,
    head_gain_h,
    wo_h,
    po_h,
    out_own,
    out_in,
    wq,
    wk,
    wv,
    wg,
    pq,
    pk,
    pv,
    pg,
    wo,
    po,
    norm_gain,
    head_gain,
    lam_all,
    tok_buf,
    normed,
    band_k,
    band_v,
    sq_buf,
    sg_buf,
    pg_buf,
    slide_mix,
    paired_mix,
    k_send,
    v_send,
    q_send,
    k_all,
    v_all,
    q_all,
    s_buf,
    p_buf,
    own_acc,
    own_top,
    up_acc,
    up_top,
    stat_send,
    stat_in,
    share_send,
    share_in,
    coef_send,
    coef_in,
    ret_send,
    ret_all,
    part,
    part_bf,
    w_sem,
    in_sem,
    tok_s,
    tok_r,
    lam_s,
    lam_r,
    kv_s,
    fw_s,
    kv_r,
    q_s,
    q_r,
    tail_s,
    tail_r,
    stat_s,
    stat_r,
    share_s,
    share_r,
    coef_s,
    coef_r,
    ret_s,
    ret_r,
    rs_s,
    rs_r,
):
    R, Dl = tokens.shape
    D = Dl * T
    H = k_send.shape[0]
    C = 2 * HD
    E = S // 2
    PC = E // (H * T)
    NQ = PC * T
    KB = E // NQ
    s = lax.axis_index("sp")
    t = lax.axis_index("tp")
    half = s // E
    e = lax.rem(s, E)
    ph = lax.rem(e, PC)
    th = lax.rem(e // PC, T)
    jh = e // NQ
    share = ph * T + t

    def block(k):
        return k * NQ + (share if k % 2 == 0 else NQ - 1 - share)

    my_k = e // NQ
    my_r = lax.rem(e, NQ)
    my_share = jnp.where(lax.rem(my_k, 2) == 0, my_r, NQ - 1 - my_r)
    my_p = my_share // T
    my_c = lax.rem(my_share, T)
    my_rc = lax.rem(e, T)

    def dev(sp, tp):
        return {"sp": sp, "tp": tp}

    def remote(src, dst, ss, rs, device):
        return pltpu.make_async_remote_copy(src, dst, ss, rs, device_id=device, device_id_type=MESH)

    class Send:
        def __init__(self, here, src, dst, ss, rs, device):
            self.here = here
            self.near = lambda: pltpu.make_async_copy(src, dst, rs)
            self.far = lambda: remote(src, dst, ss, rs, device)

        def start(self):
            @pl.when(self.here)
            def _():
                self.near().start()

            @pl.when(jnp.logical_not(self.here))
            def _():
                self.far().start()

        def wait_send(self):
            @pl.when(jnp.logical_not(self.here))
            def _():
                self.far().wait_send()

    def arrived(ref, ss, rs):
        remote(ref, ref, ss, rs, dev(lax.rem(s + 1, S), t)).wait_recv()

    barrier = pltpu.get_barrier_semaphore()

    def greet(d, _):
        f = lax.rem(s * T + t + d, S * T)
        pl.semaphore_signal(barrier, inc=1, device_id=dev(f // T, lax.rem(f, T)), device_id_type=MESH)
        return 0

    own_tok = pltpu.make_async_copy(tokens, tok_buf.at[t], in_sem.at[0])
    own_tok.start()
    lax.fori_loop(1, S * T, greet, 0)
    small = [
        pltpu.make_async_copy(gain_h, norm_gain, in_sem.at[1]),
        pltpu.make_async_copy(head_gain_h, head_gain, in_sem.at[2]),
        pltpu.make_async_copy(lam_h, lam_all.at[t], in_sem.at[3]),
    ]
    for cp in small:
        cp.start()
    pairs = [(pk_h, pk), (pq_h, pq), (pv_h, pv), (wk_h, wk), (wv_h, wv), (wq_h, wq), (wg_h, wg), (pg_h, pg), (wo_h, wo), (po_h, po)]
    loads = [pltpu.make_async_copy(a, b, w_sem.at[i]) for i, (a, b) in enumerate(pairs)]
    with jax.named_scope("own_tok"):
        own_tok.wait()
        for cp in small:
            cp.wait()
    for cp in loads:
        cp.start()
    with jax.named_scope("barrier"):
        pl.semaphore_wait(barrier, S * T - 1)

    Rn = R // 2

    def tok_copy(dt, h):
        at = tok_buf.at[t, pl.ds(h * Rn, Rn)]
        return remote(at, at, tok_s.at[dt, h], tok_r.at[dt, h], dev(s, lax.rem(t + dt, T)))

    def tok_in(dt, h):
        at = tok_buf.at[lax.rem(t + T - dt, T), pl.ds(h * Rn, Rn)]
        return remote(at, at, tok_s.at[dt, h], tok_r.at[dt, h], dev(s, lax.rem(t + dt, T)))

    def lam_copy(dt):
        at = lam_all.at[t]
        return remote(at, at, lam_s.at[dt], lam_r.at[dt], dev(s, lax.rem(t + dt, T)))

    def lam_in(dt):
        at = lam_all.at[lax.rem(t + T - dt, T)]
        return remote(at, at, lam_s.at[dt], lam_r.at[dt], dev(s, lax.rem(t + dt, T)))

    for h in range(2):
        for dt in range(1, T):
            tok_copy(dt, h).start()
    for dt in range(1, T):
        lam_copy(dt).start()

    NB = 32

    def norm_rows(i, _):
        rows = pl.ds(pl.multiple_of(i * NB, NB), NB)
        xs = [tok_buf[k, rows, :].astype(F32) for k in range(T)]
        total = sum(jnp.sum(x * x, axis=-1, keepdims=True) for x in xs)
        r = lax.rsqrt(total * (1.0 / D) + norm_eps)
        for k in range(T):
            cols = slice(k * Dl, (k + 1) * Dl)
            normed[rows, cols] = (xs[k] * r * norm_gain[:, cols]).astype(BF16)
        return 0

    for h in range(2):
        with jax.named_scope(f"tok{h}"):
            for dt in range(1, T):
                tok_in(dt, h).wait_recv()
        with jax.named_scope(f"norm{h}"):
            lax.fori_loop(h * Rn // NB, (h + 1) * Rn // NB, norm_rows, 0)

    def project(i, store):
        loads[i].wait()
        w = pairs[i][1]
        cols = w.shape[1]
        tile = min(256, cols)
        for c in range(0, cols, tile):
            r = jnp.dot(normed[...], w[:, c : c + tile], preferred_element_type=F32).astype(BF16)
            store(c, tile, r)

    def by_head(put):
        def store(c, tile, r):
            for o in range(0, tile, C):
                put((c + o) // C, r[:, o : o + C])

        return store

    scale = HD**-0.5

    def put_k(j, r):
        k_send[j] = r

    def put_v(j, r):
        v_send[j] = r.T

    def put_q(j, r):
        q_send[j] = (r * scale).T

    def kv_copies(i):
        src, dst = (k_send, k_all) if i == 0 else (v_send, v_all)
        out = []
        for j in range(H):
            for p in range(PC):
                to = (j * T + t) * PC + p
                here = (to == e) & (my_rc == t)
                out.append(
                    Send(here, src.at[j], dst.at[e], kv_s.at[i, j * PC + p], kv_r.at[i, e], dev(half * E + to, my_rc))
                )
        return out

    def q_copies(i):
        out = []
        for j in range(H):
            to = (j * T + t) * PC + my_p
            here = (i == 0) & (to == e) & (my_c == t)
            base = half * E if i == 0 else 0
            out.append(
                Send(here, q_send.at[j], q_all.at[i, my_k], q_s.at[i, j], q_r.at[i, my_k], dev(base + to, my_c))
            )
        return out

    def slot(i, n):
        return (k_all if i == 0 else v_all).at[n], kv_r.at[i, n]

    def relay_block(n):
        return lax.rem(e // T + n, E // T) * T + t

    def relay_copy(i, n, dt):
        b = relay_block(n)
        ref, rs = slot(i, b)
        return remote(ref, ref, fw_s.at[i, n, dt], rs, dev(s, lax.rem(t + dt, T)))

    def relay(i, first, last):
        def one(n, _):
            ref, rs = slot(i, relay_block(n))
            arrived(ref, fw_s.at[i, n, 0], rs)
            for dt in range(1, T):
                relay_copy(i, n, dt).start()
            return 0

        with jax.named_scope(f"relay{i}"):
            lax.fori_loop(first, last, one, 0)

    with jax.named_scope("proj_k"):
        project(0, by_head(put_k))
        for cp in kv_copies(0):
            cp.start()
    with jax.named_scope("proj_q"):
        project(1, by_head(put_q))

        @pl.when(half == 1)
        def _():
            for cp in q_copies(1):
                cp.start()

        for cp in q_copies(0):
            cp.start()

    with jax.named_scope("proj_v"):
        project(2, by_head(put_v))
        for cp in kv_copies(1):
            cp.start()

    def into(ref, first=0):
        def store(c, tile, r):
            ref[first:, c : c + tile] = r

        return store

    with jax.named_scope("proj_band"):
        project(3, into(band_k, WINDOW))
        project(4, into(band_v, WINDOW))

    def tails():
        return [
            remote(
                b.at[pl.ds(R, WINDOW)], b.at[pl.ds(0, WINDOW)], tail_s.at[i], tail_r.at[i], dev(lax.rem(s + 1, S), t)
            )
            for i, b in enumerate((band_k, band_v))
        ]

    @pl.when(s < S - 1)
    def _():
        for cp in tails():
            cp.start()

    @pl.when(s == 0)
    def _():
        band_k[0:WINDOW] = jnp.zeros((WINDOW, band_k.shape[1]), BF16)
        band_v[0:WINDOW] = jnp.zeros((WINDOW, band_v.shape[1]), BF16)

    n_relay = E // T
    relay(0, 0, n_relay // 2)
    with jax.named_scope("proj_sq"):
        project(5, into(sq_buf))
    relay(0, n_relay // 2, n_relay)

    def peers(i):
        def one(n, _):
            b = lax.rem(e // T + n // (T - 1), E // T) * T + lax.rem(t + 1 + lax.rem(n, T - 1), T)
            ref, rs = slot(i, b)
            arrived(ref, fw_s.at[i, 0, 0], rs)
            return 0

        with jax.named_scope(f"peers{i}"):
            lax.fori_loop(0, n_relay * (T - 1), one, 0)

    peers(0)
    with jax.named_scope("q_wait"):
        for k in range(KB):
            arrived(q_all.at[0, k], q_s.at[0, 0], q_r.at[0, k])

    row = lax.broadcasted_iota(jnp.int32, (C, R), 0)
    ones = jnp.ones((ONES, R), BF16)

    def scores(q, bs, first_masked, mine):
        zero = jnp.zeros_like(q)
        q2 = jnp.concatenate([jnp.where(row < HD, q, zero), jnp.where(row < HD, zero, q)], axis=1)
        top8 = None
        for i, b in enumerate(bs):
            st = jnp.dot(k_all[b], q2, preferred_element_type=F32)
            if b >= first_masked:
                ki = lax.broadcasted_iota(jnp.int32, (R, 2 * R), 0)
                qi = lax.rem(lax.broadcasted_iota(jnp.int32, (R, 2 * R), 1), R)
                st = jnp.where(qi - ki >= (b - mine) * R, st, -jnp.inf)
            s_buf[i] = st
            m8 = jnp.max(st.reshape(R // 8, 8, 2 * R), axis=0)
            top8 = m8 if top8 is None else jnp.maximum(top8, m8)
        return jnp.max(top8, axis=0, keepdims=True)

    def chunks_of(n):
        return [range(f, min(n, f + CHUNK)) for f in range(0, n, CHUNK)]

    def stats(k):
        total = top = None
        for bs in chunks_of(NQ * (k + 1)):
            old = top
            top = scores(q_all[0, k], bs, NQ * k, block(k))
            if old is not None:
                top = jnp.maximum(top, old)
                total = total * jnp.exp(old - top)
            for i in range(len(bs)):
                p = jnp.sum(jnp.exp(s_buf[i] - top).reshape(R // 8, 8, 2 * R), axis=0)
                total = p if total is None else total + p
        stat_send[k, 0:1] = top
        stat_send[k, 1:2] = jnp.sum(total, axis=0, keepdims=True)

    other = dev((1 - half) * E + e, t)

    def stat_copy():
        return remote(stat_send, stat_in, stat_s, stat_r, other)

    low = half == 0

    @pl.when(jnp.logical_not(low))
    def _():
        with jax.named_scope("stats"):
            for k in range(KB):
                stats(k)
            stat_copy().start()

    with jax.named_scope("proj_sg"):
        project(6, into(sg_buf))
    with jax.named_scope("proj_pg"):
        project(7, into(pg_buf))
    relay(1, 0, n_relay // 2)

    with jax.named_scope("tail"):

        @pl.when(s > 0)
        def _():
            for cp in tails():
                cp.wait_recv()

    kv_heads = band_k.shape[1] // HD
    group = sq_buf.shape[1] // band_k.shape[1]
    W = WINDOW
    blocks = R // W
    key_i = lax.broadcasted_iota(jnp.int32, (2 * W, group * W), 0)
    qry_i = lax.rem(lax.broadcasted_iota(jnp.int32, (2 * W, group * W), 1), W)
    lane_head = lax.broadcasted_iota(jnp.int32, (1, group * W), 1) // W
    dist = qry_i - key_i + W
    in_band = (dist >= 0) & (dist < W)

    def window_block(b):
        r0 = b * W
        ok = in_band & (s * R + r0 - W + key_i >= 0)
        for h in range(kv_heads):
            k = band_k[r0 : r0 + 2 * W, h * HD : (h + 1) * HD]
            v = band_v[r0 : r0 + 2 * W, h * HD : (h + 1) * HD]
            q = jnp.concatenate(
                [sq_buf[r0 : r0 + W, (h * group + g) * HD : (h * group + g + 1) * HD] for g in range(group)], axis=0
            )
            sc = jnp.where(ok, dot_nt(k, q) * scale, -jnp.inf)
            sk = jnp.full((1, group * W), sink[0, h * group], F32)
            for g in range(1, group):
                sk = jnp.where(lane_head == g, sink[0, h * group + g], sk)
            top = jnp.maximum(jnp.max(sc, axis=0, keepdims=True), sk)
            w = jnp.exp(sc - top)
            den = jnp.sum(w, axis=0, keepdims=True) + jnp.exp(sk - top)
            probs = (w * (1.0 / den)).astype(BF16)
            o = dot_tn(v, probs)
            o = jnp.concatenate([o[:, g * W : (g + 1) * W] for g in range(group)], axis=0).T
            cols = slice(h * group * HD, (h + 1) * group * HD)
            gate = sg_buf[r0 : r0 + W, cols].astype(F32)
            slide_mix[r0 : r0 + W, cols] = (o * silu(gate)).astype(BF16)

    for b in range(blocks):
        with jax.named_scope(f"win{b}"):
            window_block(b)
        if b == 0:
            relay(1, n_relay // 2, n_relay)

    NT = min(512, D)
    with jax.named_scope("wo"):
        loads[8].wait()
        for c in range(0, D, NT):
            part[:, c : c + NT] = jnp.dot(slide_mix[...], wo[:, c : c + NT], preferred_element_type=F32)

    for dt in range(1, T):
        lam_in(dt).wait_recv()
    lam_lane = lax.broadcasted_iota(jnp.int32, (1, H), 1)
    lam = jnp.sum(jnp.where(lam_lane == jh, lam_all[th], 0.0), axis=1, keepdims=True)

    peers(1)

    def attend(q, n, first_masked, mine, acc_ref, top_ref):
        for bs in chunks_of(n):
            top = scores(q, bs, first_masked, mine)
            if bs[0]:
                old = top_ref[...]
                top = jnp.maximum(top, old)
            for i in range(len(bs)):
                p_buf[i] = jnp.exp(s_buf[i] - top).astype(BF16)
            v = jnp.concatenate([v_all[b] for b in bs], axis=1)
            v = jnp.concatenate([v, jnp.concatenate([ones] * len(bs), axis=1)], axis=0)
            acc = jnp.dot(v, p_buf[0 : len(bs)].reshape(len(bs) * R, 2 * R), preferred_element_type=F32)
            if bs[0]:
                acc = acc + acc_ref[...] * jnp.exp(old - top)
            acc_ref[...] = acc
            top_ref[...] = top

    def own_block(k):
        with jax.named_scope(f"own{k}"):
            attend(q_all[0, k], NQ * (k + 1), NQ * k, block(k), own_acc.at[k], own_top.at[k])

    def up_block(k, _):
        with jax.named_scope("up"):
            arrived(q_all.at[1, k], q_s.at[1, 0], q_r.at[1, k])
            attend(q_all[1, k], E, E, 0, up_acc.at[k], up_top.at[k])
        return 0

    def share_copy(k):
        return remote(share_send.at[k], share_in.at[k], share_s.at[k], share_r.at[k], other)

    def coef_copy(k):
        return remote(coef_send.at[k], coef_in.at[k], coef_s.at[k], coef_r.at[k], other)

    def share_block(k, _):
        with jax.named_scope("share"):
            top = up_top[k]
            far_top = stat_in[k, 0:1]
            both = jnp.maximum(top, far_top)
            f = jnp.exp(top - both)
            far_f = jnp.exp(far_top - both)
            inv = 1.0 / (up_acc[k, C : C + 1] * f + stat_in[k, 1:2] * far_f)
            coef_send[k] = jnp.broadcast_to(far_f * inv, (8, 2 * R))
            a = up_acc[k, 0:C] * (f * inv)
            share_send[k] = (a[:, 0:R] - lam * a[:, R:]).astype(BF16)
            coef_copy(k).start()
            share_copy(k).start()
        return 0

    def ret_copy(k):
        b = block(k)
        here = (b == e) & (th == t)
        return Send(here, ret_send.at[k], ret_all.at[jh], ret_s.at[k], ret_r.at[jh], dev(half * E + b, th))

    def give_back(k, d):
        sq = jnp.mean(d * d, axis=0, keepdims=True)
        y = (d * (lax.rsqrt(sq + norm_eps) * head_scale)).T * head_gain[...]
        ret_send[k] = y.astype(BF16)
        ret_copy(k).start()

    def finish_low(k):
        with jax.named_scope(f"fin{k}"):
            a = own_acc[k, 0:C] * (1.0 / own_acc[k, C : C + 1])
            give_back(k, a[:, 0:R] - lam * a[:, R:])

    def finish_high(k):
        with jax.named_scope(f"share_wait{k}"):
            arrived(coef_in.at[k], coef_s.at[k], coef_r.at[k])
            arrived(share_in.at[k], share_s.at[k], share_r.at[k])
        a = own_acc[k, 0:C] * coef_in[k, 0:1]
        give_back(k, a[:, 0:R] - lam * a[:, R:] + share_in[k].astype(F32))

    @pl.when(low)
    def _():
        up_block(0, 0)
        with jax.named_scope("stat_wait"):
            arrived(stat_in, stat_s, stat_r)
        share_block(0, 0)

        def both(k, _):
            up_block(k, 0)
            share_block(k, 0)
            return 0

        lax.fori_loop(1, KB, both, 0)

    for k in range(KB):
        own_block(k)

        @pl.when(low)
        def _(k=k):
            finish_low(k)

    @pl.when(jnp.logical_not(low))
    def _():
        for k in range(KB):
            finish_high(k)

    with jax.named_scope("ret_wait"):
        for j in range(H):
            arrived(ret_all.at[j], ret_s.at[0], ret_r.at[j])
    for j in range(H):
        cols = slice(j * C, (j + 1) * C)
        gate = pg_buf[:, cols].astype(F32)
        paired_mix[:, cols] = (ret_all[j].astype(F32) * silu(gate)).astype(BF16)
    loads[9].wait()
    Rt = R // T
    chunks = range(0, D, NT)

    def rs_copy(dt, i):
        cols = pl.ds(i * NT, NT)
        return remote(
            part_bf.at[lax.rem(t + dt, T), :, cols],
            out_in.at[dt - 1, :, cols],
            rs_s.at[dt, i],
            rs_r.at[dt, i],
            dev(s, lax.rem(t + dt, T)),
        )

    def own_out(i):
        cols = pl.ds(i * NT, NT)
        return pltpu.make_async_copy(part_bf.at[t, :, cols], out_own.at[:, cols], rs_s.at[0, i])

    with jax.named_scope("po"):
        for i, c in enumerate(chunks):
            r = part[:, c : c + NT] + jnp.dot(paired_mix[...], po[:, c : c + NT], preferred_element_type=F32)
            r = r.astype(BF16)
            for k in range(T):
                part_bf[k, :, c : c + NT] = r[k * Rt : (k + 1) * Rt]
            for dt in range(1, T):
                rs_copy(dt, i).start()
            own_out(i).start()

    with jax.named_scope("drain"):
        for h in range(2):
            for dt in range(1, T):
                tok_copy(dt, h).wait_send()
        for dt in range(1, T):
            lam_copy(dt).wait_send()
        for i in range(2):
            for cp in kv_copies(i):
                cp.wait_send()

            def fw_drain(n, _, i=i):
                for dt in range(1, T):
                    relay_copy(i, n, dt).wait_send()
                return 0

            lax.fori_loop(0, n_relay, fw_drain, 0)
        for cp in q_copies(0):
            cp.wait_send()

        @pl.when(half == 1)
        def _():
            for cp in q_copies(1):
                cp.wait_send()
            stat_copy().wait_send()

        @pl.when(low)
        def _():
            for k in range(KB):
                coef_copy(k).wait_send()
                share_copy(k).wait_send()

        for k in range(KB):
            ret_copy(k).wait_send()

        @pl.when(s < S - 1)
        def _():
            for cp in tails():
                cp.wait_send()

    with jax.named_scope("rs_wait"):
        for i in range(D // NT):
            own_out(i).wait()
            for dt in range(1, T):
                rs_copy(dt, i).wait_send()
                rs_copy(dt, i).wait_recv()


def per_device(S, T, tokens, norm_gain, wq, wk, wv, wg, sink, pq, pk, pv, pg, lam, head_gain, wo, po):
    R, Dl = tokens.shape
    D = Dl * T
    A = wq.shape[1]
    KC = wk.shape[1]
    B = pq.shape[1]
    C = 2 * HD
    H = B // C
    E = S // 2
    PC = E // (H * T)
    KB = E // (PC * T)
    if S % 2 or PC * H * T != E:
        raise ValueError("unsupported mesh")
    Rt = R // T
    NC = D // min(512, D)
    smem = pl.BlockSpec(memory_space=pltpu.SMEM)
    hbm = pl.BlockSpec(memory_space=pl.ANY)
    dma = pltpu.SemaphoreType.DMA
    V = pltpu.VMEM
    scratch = [V(w.shape, BF16) for w in (wq, wk, wv, wg, pq, pk, pv, pg, wo, po)]
    scratch += [
        V((1, D), F32),
        V((1, C), F32),
        V((T, 1, H), F32),
        V((T, R, Dl), BF16),
        V((R, D), BF16),
        V((WINDOW + R, KC), BF16),
        V((WINDOW + R, KC), BF16),
        V((R, A), BF16),
        V((R, A), BF16),
        V((R, B), BF16),
        V((R, A), BF16),
        V((R, B), BF16),
        V((H, R, C), BF16),
        V((H, C, R), BF16),
        V((H, C, R), BF16),
        V((E, R, C), BF16),
        V((E, C, R), BF16),
        V((2, KB, C, R), BF16),
        V((min(E, CHUNK), R, 2 * R), F32),
        V((min(E, CHUNK), R, 2 * R), BF16),
        V((KB, C + ONES, 2 * R), F32),
        V((KB, 1, 2 * R), F32),
        V((KB, C + ONES, 2 * R), F32),
        V((KB, 1, 2 * R), F32),
        V((KB, 8, 2 * R), F32),
        V((KB, 8, 2 * R), F32),
        V((KB, C, R), BF16),
        V((KB, C, R), BF16),
        V((KB, 8, 2 * R), F32),
        V((KB, 8, 2 * R), F32),
        V((KB, R, C), BF16),
        V((H, R, C), BF16),
        V((R, D), F32),
        V((T, Rt, D), BF16),
        dma((10,)),
        dma((4,)),
        dma((T, 2)),
        dma((T, 2)),
        dma((T,)),
        dma((T,)),
        dma((2, H * PC)),
        dma((2, E // T, T)),
        dma((2, E)),
        dma((2, H)),
        dma((2, KB)),
        dma((2,)),
        dma((2,)),
        dma,
        dma,
        dma((KB,)),
        dma((KB,)),
        dma((KB,)),
        dma((KB,)),
        dma((KB,)),
        dma((H,)),
        dma((T, NC)),
        dma((T, NC)),
    ]
    own, others = pl.pallas_call(
        functools.partial(kernel, S, T),
        out_shape=[jax.ShapeDtypeStruct((Rt, D), BF16), jax.ShapeDtypeStruct((T - 1, Rt, D), BF16)],
        in_specs=[hbm, hbm, hbm, hbm, hbm, hbm, smem, hbm, hbm, hbm, hbm, hbm, hbm, hbm, hbm],
        out_specs=[hbm, hbm],
        scratch_shapes=scratch,
        compiler_params=pltpu.CompilerParams(
            collective_id=0, has_side_effects=True, vmem_limit_bytes=60 * 1024 * 1024
        ),
        name="layer",
    )(
        tokens,
        norm_gain.reshape(1, D),
        wq,
        wk,
        wv,
        wg,
        sink.reshape(1, -1),
        pq,
        pk,
        pv,
        pg,
        lam.reshape(1, -1),
        head_gain.reshape(1, -1),
        wo,
        po,
    )
    return (own.astype(F32) + jnp.sum(others.astype(F32), axis=0)).astype(BF16)


def solution(mesh):
    S, T = mesh.shape["sp"], mesh.shape["tp"]
    in_specs = (
        P("sp", "tp"),
        P(),
        P(None, "tp"),
        P(None, "tp"),
        P(None, "tp"),
        P(None, "tp"),
        P("tp"),
        P(None, "tp"),
        P(None, "tp"),
        P(None, "tp"),
        P(None, "tp"),
        P("tp"),
        P(),
        P("tp", None),
        P("tp", None),
    )
    return jax.shard_map(
        functools.partial(per_device, S, T),
        mesh=mesh,
        in_specs=in_specs,
        out_specs=P(("sp", "tp"), None),
        check_vma=False,
    )
```

time: 62.8 us -> 55.7 us (0.89)
  the two profiles are of different devices: /device:TPU:1 before, /device:TPU:25 now
where the time goes in v1:
time: 55.7 us; the launch traced here: 55.6 us
  Pallas kernels  53.4 us (96%)
  other arithmetic  2.12 us (4%)
    pallas_call x1, Pallas kernels, per_device(): pl.pallas_call(functools.partial(kernel, S, T), out_shape=[jax.ShapeDtype...  53.4 us
    convert_element_type x1, other arithmetic, per_device(): return (own.astype(F32) + jnp.sum(others.astype(F32), axis=0)).astype(BF16)  2.12 us

profile of v1, /device:TPU:25, one launch (start us, length us, event | category | flops | bytes accessed | tf_op | source)
XLA Modules:
  0.0 55.6 jit_solution(746112390781697642)
XLA Ops:
  0.0 53.4 %layer.1 = (bf16[128,2048]{1,0:T(8,128)(2,1)}, bf16[1,128,2048]{2,1,0:T(8,128)(2,1)}) custom-call(bf16[256,1024]{1,0:T(8,128)(2,1)} %tokens.1, f32[1,2048]{1,0:T(1,128)} %bitcast.7, bf16[2048,512]{1,0:T(8,128)(2,1)} %wq_h.1, bf16[2048,256]{1,0:T(8,128)(2,1)} %wk_h.1, bf16[2048,256]{1,0:T(8,128)(2,1)} %wv_h.1, bf16[2048,512]{1,0:T(8,128)(2,1)} %wg_h.1, ...), custom_call_target="tpu_custom_call" | custom-call | tf_op jit(solution)/shard_map/layer/pallas_call | solution.py:762
  53.4 2.1 %fusion = bf16[128,2048]{1,0:T(8,128)(2,1)} fusion(bf16[128,2048]{1,0:T(8,128)(2,1)} %get-tuple-element.7, bf16[1,128,2048]{2,1,0:T(8,128)(2,1)} %get-tuple-element.8), kind=kLoop, calls=%fused_computation.1 | loop fusion | flops 1048576 | bytes 1572864 | tf_op jit(solution)/shard_map/convert_element_type | solution.py:789

commit v2 on v1

--- a/solution.py
+++ b/solution.py
@@ -128,6 +128,12 @@
     PC = E // (H * T)
     NQ = PC * T
     KB = E // NQ
+
+    def goes_up(j):
+        return False
+
+    ups = [j for j in range(H) if goes_up(j)]
+    downs = [j for j in range(H) if not goes_up(j)]
     s = lax.axis_index("sp")
     t = lax.axis_index("tp")
     half = s // E
@@ -137,8 +143,14 @@
     jh = e // NQ
     share = ph * T + t
 
+    low = half == 0
+    keys_up = functools.reduce(jnp.logical_or, [jh == j for j in ups], jh < 0)
+    up_core = jnp.logical_not(low) & keys_up
+    down_core = low & jnp.logical_not(keys_up)
+    asking_core = jnp.logical_not(low) & jnp.logical_not(keys_up)
+
     def block(k):
-        return k * NQ + (share if k % 2 == 0 else NQ - 1 - share)
+        return k * NQ + jnp.where(lax.rem(k, 2) == 0, share, NQ - 1 - share)
 
     my_k = e // NQ
     my_r = lax.rem(e, NQ)
@@ -193,7 +205,7 @@
     ]
     for cp in small:
         cp.start()
-    pairs = [(pk_h, pk), (pq_h, pq), (pv_h, pv), (wk_h, wk), (wv_h, wv), (wq_h, wq), (wg_h, wg), (pg_h, pg), (wo_h, wo), (po_h, po)]
+    pairs = [(pk_h, pk), (pv_h, pv), (pq_h, pq), (wk_h, wk), (wv_h, wv), (wq_h, wq), (wg_h, wg), (pg_h, pg), (wo_h, wo), (po_h, po)]
     loads = [pltpu.make_async_copy(a, b, w_sem.at[i]) for i, (a, b) in enumerate(pairs)]
     with jax.named_scope("own_tok"):
         own_tok.wait()
@@ -274,21 +286,21 @@
     def put_q(j, r):
         q_send[j] = (r * scale).T
 
-    def kv_copies(i):
+    def kv_copies(i, up, heads):
         src, dst = (k_send, k_all) if i == 0 else (v_send, v_all)
         out = []
-        for j in range(H):
+        for j in heads:
             for p in range(PC):
                 to = (j * T + t) * PC + p
-                here = (to == e) & (my_rc == t)
-                out.append(
-                    Send(here, src.at[j], dst.at[e], kv_s.at[i, j * PC + p], kv_r.at[i, e], dev(half * E + to, my_rc))
-                )
+                here = (up == 0) & (to == e) & (my_rc == t)
+                base = E if up else half * E
+                ss = kv_s.at[i, up, j * PC + p]
+                out.append(Send(here, src.at[j], dst.at[up, e], ss, kv_r.at[i, up, e], dev(base + to, my_rc)))
         return out
 
-    def q_copies(i):
+    def q_copies(i, heads):
         out = []
-        for j in range(H):
+        for j in heads:
             to = (j * T + t) * PC + my_p
             here = (i == 0) & (to == e) & (my_c == t)
             base = half * E if i == 0 else 0
@@ -297,47 +309,89 @@
             )
         return out
 
-    def slot(i, n):
-        return (k_all if i == 0 else v_all).at[n], kv_r.at[i, n]
-
-    def relay_block(n):
-        return lax.rem(e // T + n, E // T) * T + t
-
-    def relay_copy(i, n, dt):
-        b = relay_block(n)
-        ref, rs = slot(i, b)
-        return remote(ref, ref, fw_s.at[i, n, dt], rs, dev(s, lax.rem(t + dt, T)))
-
-    def relay(i, first, last):
+    n_relay = E // T
+
+    def slot(i, up, n):
+        return (k_all if i == 0 else v_all).at[up, n], kv_r.at[i, up, n]
+
+    def relay_block(up, n, core):
+        first = n_relay - 1 - n if up else lax.rem(e // T + n, n_relay)
+        return first * T + core
+
+    def relay_copy(i, up, n, dt):
+        ref, rs = slot(i, up, relay_block(up, n, t))
+        return remote(ref, ref, fw_s.at[i, up, n, dt], rs, dev(s, lax.rem(t + dt, T)))
+
+    def relay(i, first, last, up=0):
         def one(n, _):
-            ref, rs = slot(i, relay_block(n))
-            arrived(ref, fw_s.at[i, n, 0], rs)
+            ref, rs = slot(i, up, relay_block(up, n, t))
+            arrived(ref, fw_s.at[i, up, n, 0], rs)
             for dt in range(1, T):
-                relay_copy(i, n, dt).start()
+                relay_copy(i, up, n, dt).start()
             return 0
 
-        with jax.named_scope(f"relay{i}"):
+        with jax.named_scope(f"relay{i}{up}"):
             lax.fori_loop(first, last, one, 0)
+
+    def peers(i, first, last, up=0):
+        def one(n, _):
+            core = lax.rem(t + 1 + lax.rem(n, T - 1), T)
+            ref, rs = slot(i, up, relay_block(up, n // (T - 1), core))
+            arrived(ref, fw_s.at[i, up, 0, 0], rs)
+            return 0
+
+        with jax.named_scope(f"peers{i}{up}"):
+            lax.fori_loop(first * (T - 1), last * (T - 1), one, 0)
+
+    def begin(copies):
+        for cp in copies:
+            cp.start()
+
+    def begin(copies):
+        for cp in copies:
+            cp.start()
+
+    high = jnp.logical_not(low)
 
     with jax.named_scope("proj_k"):
         project(0, by_head(put_k))
-        for cp in kv_copies(0):
-            cp.start()
+
+        @pl.when(high)
+        def _():
+            begin(kv_copies(0, 0, downs + ups))
+
+        @pl.when(low)
+        def _():
+            begin(kv_copies(0, 0, downs))
+
+    with jax.named_scope("proj_v"):
+        project(1, by_head(put_v))
+
+        @pl.when(low)
+        def _():
+            begin(kv_copies(1, 0, downs))
+            for i in range(2):
+                begin(kv_copies(i, 1, ups))
+
     with jax.named_scope("proj_q"):
-        project(1, by_head(put_q))
-
-        @pl.when(half == 1)
-        def _():
-            for cp in q_copies(1):
-                cp.start()
-
-        for cp in q_copies(0):
-            cp.start()
-
-    with jax.named_scope("proj_v"):
-        project(2, by_head(put_v))
-        for cp in kv_copies(1):
-            cp.start()
+        project(2, by_head(put_q))
+
+        @pl.when(high)
+        def _():
+            begin(q_copies(0, downs + ups))
+            begin(q_copies(1, downs[::-1]))
+            begin(kv_copies(1, 0, ups))
+
+    def late_sends():
+        @pl.when(low)
+        def _():
+            for i in range(2):
+                begin(kv_copies(i, 0, ups))
+            begin(q_copies(0, ups + downs))
+
+        @pl.when(high)
+        def _():
+            begin(kv_copies(1, 0, downs))
 
     def into(ref, first=0):
         def store(c, tile, r):
@@ -367,88 +421,12 @@
         band_k[0:WINDOW] = jnp.zeros((WINDOW, band_k.shape[1]), BF16)
         band_v[0:WINDOW] = jnp.zeros((WINDOW, band_v.shape[1]), BF16)
 
-    n_relay = E // T
-    relay(0, 0, n_relay // 2)
     with jax.named_scope("proj_sq"):
         project(5, into(sq_buf))
-    relay(0, n_relay // 2, n_relay)
-
-    def peers(i):
-        def one(n, _):
-            b = lax.rem(e // T + n // (T - 1), E // T) * T + lax.rem(t + 1 + lax.rem(n, T - 1), T)
-            ref, rs = slot(i, b)
-            arrived(ref, fw_s.at[i, 0, 0], rs)
-            return 0
-
-        with jax.named_scope(f"peers{i}"):
-            lax.fori_loop(0, n_relay * (T - 1), one, 0)
-
-    peers(0)
-    with jax.named_scope("q_wait"):
-        for k in range(KB):
-            arrived(q_all.at[0, k], q_s.at[0, 0], q_r.at[0, k])
-
-    row = lax.broadcasted_iota(jnp.int32, (C, R), 0)
-    ones = jnp.ones((ONES, R), BF16)
-
-    def scores(q, bs, first_masked, mine):
-        zero = jnp.zeros_like(q)
-        q2 = jnp.concatenate([jnp.where(row < HD, q, zero), jnp.where(row < HD, zero, q)], axis=1)
-        top8 = None
-        for i, b in enumerate(bs):
-            st = jnp.dot(k_all[b], q2, preferred_element_type=F32)
-            if b >= first_masked:
-                ki = lax.broadcasted_iota(jnp.int32, (R, 2 * R), 0)
-                qi = lax.rem(lax.broadcasted_iota(jnp.int32, (R, 2 * R), 1), R)
-                st = jnp.where(qi - ki >= (b - mine) * R, st, -jnp.inf)
-            s_buf[i] = st
-            m8 = jnp.max(st.reshape(R // 8, 8, 2 * R), axis=0)
-            top8 = m8 if top8 is None else jnp.maximum(top8, m8)
-        return jnp.max(top8, axis=0, keepdims=True)
-
-    def chunks_of(n):
-        return [range(f, min(n, f + CHUNK)) for f in range(0, n, CHUNK)]
-
-    def stats(k):
-        total = top = None
-        for bs in chunks_of(NQ * (k + 1)):
-            old = top
-            top = scores(q_all[0, k], bs, NQ * k, block(k))
-            if old is not None:
-                top = jnp.maximum(top, old)
-                total = total * jnp.exp(old - top)
-            for i in range(len(bs)):
-                p = jnp.sum(jnp.exp(s_buf[i] - top).reshape(R // 8, 8, 2 * R), axis=0)
-                total = p if total is None else total + p
-        stat_send[k, 0:1] = top
-        stat_send[k, 1:2] = jnp.sum(total, axis=0, keepdims=True)
-
-    other = dev((1 - half) * E + e, t)
-
-    def stat_copy():
-        return remote(stat_send, stat_in, stat_s, stat_r, other)
-
-    low = half == 0
-
-    @pl.when(jnp.logical_not(low))
-    def _():
-        with jax.named_scope("stats"):
-            for k in range(KB):
-                stats(k)
-            stat_copy().start()
-
     with jax.named_scope("proj_sg"):
         project(6, into(sg_buf))
     with jax.named_scope("proj_pg"):
         project(7, into(pg_buf))
-    relay(1, 0, n_relay // 2)
-
-    with jax.named_scope("tail"):
-
-        @pl.when(s > 0)
-        def _():
-            for cp in tails():
-                cp.wait_recv()
 
     kv_heads = band_k.shape[1] // HD
     group = sq_buf.shape[1] // band_k.shape[1]
@@ -483,50 +461,118 @@
             gate = sg_buf[r0 : r0 + W, cols].astype(F32)
             slide_mix[r0 : r0 + W, cols] = (o * silu(gate)).astype(BF16)
 
-    for b in range(blocks):
-        with jax.named_scope(f"win{b}"):
-            window_block(b)
-        if b == 0:
-            relay(1, n_relay // 2, n_relay)
-
-    NT = min(512, D)
-    with jax.named_scope("wo"):
-        loads[8].wait()
-        for c in range(0, D, NT):
-            part[:, c : c + NT] = jnp.dot(slide_mix[...], wo[:, c : c + NT], preferred_element_type=F32)
+    def other_windows():
+        for b in range(1, blocks):
+            with jax.named_scope(f"win{b}"):
+                window_block(b)
+
+    pl.when(low)(other_windows)
+    late_sends()
+    relay(0, 0, n_relay)
+    peers(0, 0, n_relay)
+
+    def queries():
+        with jax.named_scope("q_wait"):
+            for k in range(KB):
+                arrived(q_all.at[0, k], q_s.at[0, 0], q_r.at[0, k])
+
+    pl.when(jnp.logical_not(low))(queries)
+    row = lax.broadcasted_iota(jnp.int32, (C, R), 0)
+    ones = jnp.ones((ONES, R), BF16)
+
+    def scores(q, up, bs, first_masked, mine):
+        zero = jnp.zeros_like(q)
+        q2 = jnp.concatenate([jnp.where(row < HD, q, zero), jnp.where(row < HD, zero, q)], axis=1)
+        top8 = None
+        for i, b in enumerate(bs):
+            st = jnp.dot(k_all[up, b], q2, preferred_element_type=F32)
+            if b >= first_masked:
+                ki = lax.broadcasted_iota(jnp.int32, (R, 2 * R), 0)
+                qi = lax.rem(lax.broadcasted_iota(jnp.int32, (R, 2 * R), 1), R)
+                st = jnp.where(qi - ki >= (b - mine) * R, st, -jnp.inf)
+            s_buf[i] = st
+            m8 = jnp.max(st.reshape(R // 8, 8, 2 * R), axis=0)
+            top8 = m8 if top8 is None else jnp.maximum(top8, m8)
+        return jnp.max(top8, axis=0, keepdims=True)
+
+    def chunks_of(n):
+        return [range(f, min(n, f + CHUNK)) for f in range(0, n, CHUNK)]
+
+    def stats(k):
+        total = top = None
+        for bs in chunks_of(NQ * (k + 1)):
+            old = top
+            top = scores(q_all[0, k], 0, bs, NQ * k, block(k))
+            if old is not None:
+                top = jnp.maximum(top, old)
+                total = total * jnp.exp(old - top)
+            for i in range(len(bs)):
+                p = jnp.sum(jnp.exp(s_buf[i] - top).reshape(R // 8, 8, 2 * R), axis=0)
+                total = p if total is None else total + p
+        stat_send[k, 0:1] = top
+        stat_send[k, 1:2] = jnp.sum(total, axis=0, keepdims=True)
+
+    other = dev((1 - half) * E + e, t)
+
+    def stat_copy():
+        return remote(stat_send, stat_in, stat_s, stat_r, other)
+
+    @pl.when(asking_core)
+    def _():
+        with jax.named_scope("stats"):
+            for k in range(KB):
+                stats(k)
+            stat_copy().start()
+
+    pl.when(high)(other_windows)
+
+    def values():
+        relay(1, 0, n_relay)
+        peers(1, 0, n_relay)
+
+    pl.when(jnp.logical_not(up_core))(values)
 
     for dt in range(1, T):
         lam_in(dt).wait_recv()
     lam_lane = lax.broadcasted_iota(jnp.int32, (1, H), 1)
     lam = jnp.sum(jnp.where(lam_lane == jh, lam_all[th], 0.0), axis=1, keepdims=True)
 
-    peers(1)
-
-    def attend(q, n, first_masked, mine, acc_ref, top_ref):
-        for bs in chunks_of(n):
-            top = scores(q, bs, first_masked, mine)
-            if bs[0]:
+    def attend(q, up, parts, first_masked, mine, acc_ref, top_ref, fresh):
+        for bs in parts:
+            top = scores(q, up, bs, first_masked, mine)
+            if not fresh:
                 old = top_ref[...]
                 top = jnp.maximum(top, old)
             for i in range(len(bs)):
                 p_buf[i] = jnp.exp(s_buf[i] - top).astype(BF16)
-            v = jnp.concatenate([v_all[b] for b in bs], axis=1)
+            v = jnp.concatenate([v_all[up, b] for b in bs], axis=1)
             v = jnp.concatenate([v, jnp.concatenate([ones] * len(bs), axis=1)], axis=0)
             acc = jnp.dot(v, p_buf[0 : len(bs)].reshape(len(bs) * R, 2 * R), preferred_element_type=F32)
-            if bs[0]:
+            if not fresh:
                 acc = acc + acc_ref[...] * jnp.exp(old - top)
             acc_ref[...] = acc
             top_ref[...] = top
+            fresh = False
 
     def own_block(k):
         with jax.named_scope(f"own{k}"):
-            attend(q_all[0, k], NQ * (k + 1), NQ * k, block(k), own_acc.at[k], own_top.at[k])
-
-    def up_block(k, _):
-        with jax.named_scope("up"):
+            attend(q_all[0, k], 0, chunks_of(NQ * (k + 1)), NQ * k, block(k), own_acc.at[k], own_top.at[k], False)
+
+    def down_block(k, _):
+        with jax.named_scope("down"):
             arrived(q_all.at[1, k], q_s.at[1, 0], q_r.at[1, k])
-            attend(q_all[1, k], E, E, 0, up_acc.at[k], up_top.at[k])
+            attend(q_all[1, k], 0, chunks_of(E), E, 0, up_acc.at[k], up_top.at[k], True)
         return 0
+
+    def upper(parts, fresh, last):
+        def one(k, _):
+            with jax.named_scope("upper"):
+                attend(q_all[0, k], 1, parts, E, 0, own_acc.at[k], own_top.at[k], fresh)
+                if last:
+                    finish_low(k)
+            return 0
+
+        lax.fori_loop(0, KB, one, 0)
 
     def share_copy(k):
         return remote(share_send.at[k], share_in.at[k], share_s.at[k], share_r.at[k], other)
@@ -561,7 +607,7 @@
         ret_copy(k).start()
 
     def finish_low(k):
-        with jax.named_scope(f"fin{k}"):
+        with jax.named_scope("fin"):
             a = own_acc[k, 0:C] * (1.0 / own_acc[k, C : C + 1])
             give_back(k, a[:, 0:R] - lam * a[:, R:])
 
@@ -572,28 +618,79 @@
         a = own_acc[k, 0:C] * coef_in[k, 0:1]
         give_back(k, a[:, 0:R] - lam * a[:, R:] + share_in[k].astype(F32))
 
-    @pl.when(low)
+    @pl.when(down_core)
     def _():
-        up_block(0, 0)
+        ready = 1
+        lax.fori_loop(0, ready, down_block, 0)
         with jax.named_scope("stat_wait"):
             arrived(stat_in, stat_s, stat_r)
-        share_block(0, 0)
-
-        def both(k, _):
-            up_block(k, 0)
+        lax.fori_loop(0, ready, share_block, 0)
+        for k in range(ready, KB):
+            down_block(k, 0)
             share_block(k, 0)
-            return 0
-
-        lax.fori_loop(1, KB, both, 0)
+
+    pl.when(low)(queries)
+    @pl.when(jnp.logical_not(up_core))
+    def _():
+        own_acc[...] = jnp.zeros(own_acc.shape, F32)
+        own_top[...] = jnp.full(own_top.shape, -1e30, F32)
+
+    NT = min(512, D)
+
+    def first_window():
+        with jax.named_scope("tail"):
+
+            @pl.when(s > 0)
+            def _():
+                for cp in tails():
+                    cp.wait_recv()
+
+        with jax.named_scope("win0"):
+            window_block(0)
+        with jax.named_scope("wo"):
+            loads[8].wait()
+            for c in range(0, D, NT):
+                part[:, c : c + NT] = jnp.dot(slide_mix[...], wo[:, c : c + NT], preferred_element_type=F32)
+
+    n_near = n_relay // 2
+    near, far = range((n_relay - n_near) * T, E), range(0, (n_relay - n_near) * T)
+    if ups:
+
+        @pl.when(up_core)
+        def _():
+            for i in range(2):
+                relay(i, 0, n_near, 1)
+            for i in range(2):
+                peers(i, 0, n_near, 1)
+            upper([near], True, False)
+            first_window()
+            values()
 
     for k in range(KB):
+        if k == KB // 2 and ups:
+
+            @pl.when(up_core)
+            def _():
+                for i in range(2):
+                    relay(i, n_near, n_relay, 1)
+
         own_block(k)
 
         @pl.when(low)
         def _(k=k):
             finish_low(k)
 
-    @pl.when(jnp.logical_not(low))
+    if ups:
+
+        @pl.when(up_core)
+        def _():
+            for i in range(2):
+                peers(i, n_near, n_relay, 1)
+            upper([far], False, True)
+
+    pl.when(jnp.logical_not(up_core))(first_window)
+
+    @pl.when(asking_core)
     def _():
         for k in range(KB):
             finish_high(k)
@@ -639,26 +736,41 @@
                 tok_copy(dt, h).wait_send()
         for dt in range(1, T):
             lam_copy(dt).wait_send()
+        def relayed(up):
+            def one(n, _):
+                for i in range(2):
+                    for dt in range(1, T):
+                        relay_copy(i, up, n, dt).wait_send()
+                return 0
+
+            lax.fori_loop(0, n_relay, one, 0)
+
+        relayed(0)
         for i in range(2):
-            for cp in kv_copies(i):
+            for cp in kv_copies(i, 0, range(H)):
                 cp.wait_send()
-
-            def fw_drain(n, _, i=i):
-                for dt in range(1, T):
-                    relay_copy(i, n, dt).wait_send()
-                return 0
-
-            lax.fori_loop(0, n_relay, fw_drain, 0)
-        for cp in q_copies(0):
+        for cp in q_copies(0, range(H)):
             cp.wait_send()
 
         @pl.when(half == 1)
         def _():
-            for cp in q_copies(1):
+            for cp in q_copies(1, downs):
                 cp.wait_send()
+
+        @pl.when(low)
+        def _():
+            for i in range(2):
+                for cp in kv_copies(i, 1, ups):
+                    cp.wait_send()
+
+        if ups:
+            pl.when(up_core)(lambda: relayed(1))
+
+        @pl.when(asking_core)
+        def _():
             stat_copy().wait_send()
 
-        @pl.when(low)
+        @pl.when(down_core)
         def _():
             for k in range(KB):
                 coef_copy(k).wait_send()
@@ -716,8 +828,8 @@
         V((H, R, C), BF16),
         V((H, C, R), BF16),
         V((H, C, R), BF16),
-        V((E, R, C), BF16),
-        V((E, C, R), BF16),
+        V((2, E, R, C), BF16),
+        V((2, E, C, R), BF16),
         V((2, KB, C, R), BF16),
         V((min(E, CHUNK), R, 2 * R), F32),
         V((min(E, CHUNK), R, 2 * R), BF16),
@@ -741,9 +853,9 @@
         dma((T, 2)),
         dma((T,)),
         dma((T,)),
-        dma((2, H * PC)),
-        dma((2, E // T, T)),
-        dma((2, E)),
+        dma((2, 2, H * PC)),
+        dma((2, 2, E // T, T)),
+        dma((2, 2, E)),
         dma((2, H)),
         dma((2, KB)),
         dma((2,)),

time: 55.7 us -> 51 us (0.916)
  the two profiles are of different devices: /device:TPU:25 before, /device:TPU:31 now
where the time goes in v2:
time: 51 us; the launch traced here: 50.8 us
  Pallas kernels  48.7 us (95%)
  other arithmetic  2.12 us (4%)
    pallas_call x1, Pallas kernels, per_device(): pl.pallas_call(functools.partial(kernel, S, T), out_shape=[jax.ShapeDtype...  48.7 us
    convert_element_type x1, other arithmetic, per_device(): return (own.astype(F32) + jnp.sum(others.astype(F32), axis=0)).astype(BF16)  2.12 us

profile of v2, /device:TPU:31, one launch (start us, length us, event | category | flops | bytes accessed | tf_op | source)
XLA Modules:
  0.0 50.8 jit_solution(15688628186257836030)
XLA Ops:
  0.0 48.7 %layer.1 = (bf16[128,2048]{1,0:T(8,128)(2,1)}, bf16[1,128,2048]{2,1,0:T(8,128)(2,1)}) custom-call(bf16[256,1024]{1,0:T(8,128)(2,1)} %tokens.1, f32[1,2048]{1,0:T(1,128)} %bitcast.7, bf16[2048,512]{1,0:T(8,128)(2,1)} %wq_h.1, bf16[2048,256]{1,0:T(8,128)(2,1)} %wk_h.1, bf16[2048,256]{1,0:T(8,128)(2,1)} %wv_h.1, bf16[2048,512]{1,0:T(8,128)(2,1)} %wg_h.1, ...), custom_call_target="tpu_custom_call" | custom-call | tf_op jit(solution)/shard_map/layer/pallas_call | solution.py:874
  48.7 2.1 %fusion = bf16[128,2048]{1,0:T(8,128)(2,1)} fusion(bf16[128,2048]{1,0:T(8,128)(2,1)} %get-tuple-element.7, bf16[1,128,2048]{2,1,0:T(8,128)(2,1)} %get-tuple-element.8), kind=kLoop, calls=%fused_computation.1 | loop fusion | flops 1048576 | bytes 1572864 | tf_op jit(solution)/shard_map/convert_element_type | solution.py:901

commit v3 on v2

--- a/solution.py
+++ b/solution.py
@@ -72,6 +72,7 @@
     sq_buf,
     sg_buf,
     pg_buf,
+    gate_buf,
     slide_mix,
     paired_mix,
     k_send,
@@ -257,7 +258,7 @@
             for dt in range(1, T):
                 tok_in(dt, h).wait_recv()
         with jax.named_scope(f"norm{h}"):
-            lax.fori_loop(h * Rn // NB, (h + 1) * Rn // NB, norm_rows, 0)
+            lax.fori_loop(h * Rn // NB, (h + 1) * Rn // NB, norm_rows, 0, unroll=True)
 
     def project(i, store):
         loads[i].wait()
@@ -382,16 +383,13 @@
             begin(q_copies(1, downs[::-1]))
             begin(kv_copies(1, 0, ups))
 
-    def late_sends():
-        @pl.when(low)
-        def _():
-            for i in range(2):
-                begin(kv_copies(i, 0, ups))
-            begin(q_copies(0, ups + downs))
-
-        @pl.when(high)
-        def _():
-            begin(kv_copies(1, 0, downs))
+    def late_low():
+        for i in range(2):
+            begin(kv_copies(i, 0, ups))
+        begin(q_copies(0, ups + downs))
+
+    def late_high():
+        begin(kv_copies(1, 0, downs))
 
     def into(ref, first=0):
         def store(c, tile, r):
@@ -467,7 +465,6 @@
                 window_block(b)
 
     pl.when(low)(other_windows)
-    late_sends()
     relay(0, 0, n_relay)
     peers(0, 0, n_relay)
 
@@ -509,8 +506,8 @@
             for i in range(len(bs)):
                 p = jnp.sum(jnp.exp(s_buf[i] - top).reshape(R // 8, 8, 2 * R), axis=0)
                 total = p if total is None else total + p
-        stat_send[k, 0:1] = top
-        stat_send[k, 1:2] = jnp.sum(total, axis=0, keepdims=True)
+        stat_send[2 * k] = top
+        stat_send[2 * k + 1] = jnp.sum(total, axis=0, keepdims=True)
 
     other = dev((1 - half) * E + e, t)
 
@@ -524,6 +521,7 @@
                 stats(k)
             stat_copy().start()
 
+    pl.when(high)(late_high)
     pl.when(high)(other_windows)
 
     def values():
@@ -531,6 +529,7 @@
         peers(1, 0, n_relay)
 
     pl.when(jnp.logical_not(up_core))(values)
+    pl.when(low)(late_low)
 
     for dt in range(1, T):
         lam_in(dt).wait_recv()
@@ -583,12 +582,12 @@
     def share_block(k, _):
         with jax.named_scope("share"):
             top = up_top[k]
-            far_top = stat_in[k, 0:1]
+            far_top = stat_in[2 * k]
             both = jnp.maximum(top, far_top)
             f = jnp.exp(top - both)
             far_f = jnp.exp(far_top - both)
-            inv = 1.0 / (up_acc[k, C : C + 1] * f + stat_in[k, 1:2] * far_f)
-            coef_send[k] = jnp.broadcast_to(far_f * inv, (8, 2 * R))
+            inv = 1.0 / (up_acc[k, C : C + 1] * f + stat_in[2 * k + 1] * far_f)
+            coef_send[k] = far_f * inv
             a = up_acc[k, 0:C] * (f * inv)
             share_send[k] = (a[:, 0:R] - lam * a[:, R:]).astype(BF16)
             coef_copy(k).start()
@@ -615,7 +614,7 @@
         with jax.named_scope(f"share_wait{k}"):
             arrived(coef_in.at[k], coef_s.at[k], coef_r.at[k])
             arrived(share_in.at[k], share_s.at[k], share_r.at[k])
-        a = own_acc[k, 0:C] * coef_in[k, 0:1]
+        a = own_acc[k, 0:C] * coef_in[k]
         give_back(k, a[:, 0:R] - lam * a[:, R:] + share_in[k].astype(F32))
 
     @pl.when(down_core)
@@ -695,14 +694,25 @@
         for k in range(KB):
             finish_high(k)
 
-    with jax.named_scope("ret_wait"):
-        for j in range(H):
-            arrived(ret_all.at[j], ret_s.at[0], ret_r.at[j])
-    for j in range(H):
-        cols = slice(j * C, (j + 1) * C)
-        gate = pg_buf[:, cols].astype(F32)
-        paired_mix[:, cols] = (ret_all[j].astype(F32) * silu(gate)).astype(BF16)
+    gate = pg_buf[...].astype(F32)
+    gate_buf[...] = silu(gate)
+    def gated(heads):
+        with jax.named_scope("ret_wait"):
+            for j in heads:
+                arrived(ret_all.at[j], ret_s.at[0], ret_r.at[j])
+        for j in heads:
+            cols = slice(j * C, (j + 1) * C)
+            paired_mix[:, cols] = (ret_all[j].astype(F32) * gate_buf[:, cols]).astype(BF16)
+
     loads[9].wait()
+    H1 = H // 2
+    if H1:
+        gated(range(H1))
+        for c in range(0, D, NT):
+            part[:, c : c + NT] += jnp.dot(
+                paired_mix[:, 0 : H1 * C], po[0 : H1 * C, c : c + NT], preferred_element_type=F32
+            )
+    gated(range(H1, H))
     Rt = R // T
     chunks = range(0, D, NT)
 
@@ -722,7 +732,9 @@
 
     with jax.named_scope("po"):
         for i, c in enumerate(chunks):
-            r = part[:, c : c + NT] + jnp.dot(paired_mix[...], po[:, c : c + NT], preferred_element_type=F32)
+            r = part[:, c : c + NT] + jnp.dot(
+                paired_mix[:, H1 * C :], po[H1 * C :, c : c + NT], preferred_element_type=F32
+            )
             r = r.astype(BF16)
             for k in range(T):
                 part_bf[k, :, c : c + NT] = r[k * Rt : (k + 1) * Rt]
@@ -823,6 +835,7 @@
         V((R, A), BF16),
         V((R, A), BF16),
         V((R, B), BF16),
+        V((R, B), F32),
         V((R, A), BF16),
         V((R, B), BF16),
         V((H, R, C), BF16),
@@ -837,12 +850,12 @@
         V((KB, 1, 2 * R), F32),
         V((KB, C + ONES, 2 * R), F32),
         V((KB, 1, 2 * R), F32),
-        V((KB, 8, 2 * R), F32),
-        V((KB, 8, 2 * R), F32),
+        V((2 * KB, 1, 2 * R), F32),
+        V((2 * KB, 1, 2 * R), F32),
         V((KB, C, R), BF16),
         V((KB, C, R), BF16),
-        V((KB, 8, 2 * R), F32),
-        V((KB, 8, 2 * R), F32),
+        V((KB, 1, 2 * R), F32),
+        V((KB, 1, 2 * R), F32),
         V((KB, R, C), BF16),
         V((H, R, C), BF16),
         V((R, D), F32),

time: 51 us -> 48.1 us (0.943)
  the two profiles are of different devices: /device:TPU:31 before, /device:TPU:1 now
where the time goes in v3:
time: 48.1 us; the launch traced here: 47.8 us
  Pallas kernels  45.7 us (95%)
  other arithmetic  2.12 us (4%)
    pallas_call x1, Pallas kernels, per_device(): pl.pallas_call(functools.partial(kernel, S, T), out_shape=[jax.ShapeDtype...  45.7 us
    convert_element_type x1, other arithmetic, per_device(): return (own.astype(F32) + jnp.sum(others.astype(F32), axis=0)).astype(BF16)  2.12 us

profile of v3, /device:TPU:1, one launch (start us, length us, event | category | flops | bytes accessed | tf_op | source)
XLA Modules:
  0.0 47.8 jit_solution(17312333858761888282)
XLA Ops:
  0.0 45.7 %layer.1 = (bf16[128,2048]{1,0:T(8,128)(2,1)}, bf16[1,128,2048]{2,1,0:T(8,128)(2,1)}) custom-call(bf16[256,1024]{1,0:T(8,128)(2,1)} %tokens.1, f32[1,2048]{1,0:T(1,128)} %bitcast.7, bf16[2048,512]{1,0:T(8,128)(2,1)} %wq_h.1, bf16[2048,256]{1,0:T(8,128)(2,1)} %wk_h.1, bf16[2048,256]{1,0:T(8,128)(2,1)} %wv_h.1, bf16[2048,512]{1,0:T(8,128)(2,1)} %wg_h.1, ...), custom_call_target="tpu_custom_call" | custom-call | tf_op jit(solution)/shard_map/layer/pallas_call | solution.py:887
  45.7 2.1 %fusion = bf16[128,2048]{1,0:T(8,128)(2,1)} fusion(bf16[128,2048]{1,0:T(8,128)(2,1)} %get-tuple-element.7, bf16[1,128,2048]{2,1,0:T(8,128)(2,1)} %get-tuple-element.8), kind=kLoop, calls=%fused_computation.1 | loop fusion | flops 1048576 | bytes 1572864 | tf_op jit(solution)/shard_map/convert_element_type | solution.py:914
